TPU v7x, 32 devices: a whole 2x2x4 slice. The times are simulated.
32 devices in a mesh: kv: 16 (over z, y, x), tp: 2 (over core).
Axes of the slice: x: 2, y: 2, z: 4, core: 2. Of those that a mesh axis runs over, the one named last changes fastest.
Arguments:
- stream: bfloat16 [32, 4096], P(None, 'kv'), may hold values from -32 to 32
- gain_in: bfloat16 [4096], P('kv'), may hold values from 0.099609375 to 1.8984375
- w_query: bfloat16 [4096, 2048], P('kv', 'tp'), may hold values from -0.09375 to 0.09375
- w_key: bfloat16 [4096, 2048], P('kv', 'tp'), may hold values from -0.09375 to 0.09375
- w_value: bfloat16 [4096, 2048], P('kv', 'tp'), may hold values from -0.09375 to 0.09375
- w_forget: bfloat16 [4096, 16], replicated, may hold values from -0.09375 to 0.09375
- keys_cache: bfloat16 [32, 16, 2048, 128], P(None, 'tp', 'kv'), may hold values from -136 to 136
- values_cache: bfloat16 [32, 16, 2048, 128], P(None, 'tp', 'kv'), may hold values from -6 to 6
- decay_cache: float32 [32, 16, 2048], P(None, 'tp', 'kv'), may hold values from -323 to 0
- lengths: int32 [32], replicated, may hold values from 1 to 2048, 26246 in all
- gain_att: bfloat16 [2048], P('tp'), may hold values from 0.099609375 to 1.8984375
- w_out: bfloat16 [2048, 4096], P('tp', 'kv'), may hold values from -0.125 to 0.125
- gain_mlp: bfloat16 [4096], P('kv'), may hold values from 0.099609375 to 1.8984375
- w_up: bfloat16 [4096, 16384], P('kv', 'tp'), may hold values from -0.09375 to 0.09375
- w_down: bfloat16 [16384, 4096], P('tp', 'kv'), may hold values from -0.046875 to 0.046875
Outputs:
- updated: bfloat16 [32, 4096], P(None, 'kv')
Inputs may be any that keep to these rules, and one draw needn't show every extreme that they name: `lengths`: one sequence has all 2048 positions live.
All inputs are finite; a program needn't handle non-finite values.
Results may differ from a plain program's by a relative error of at most 0.012.
The roundings to bfloat16 on the way count: a program that leaves them out, or rounds other values in their place, can miss the bound.
Values may be sent and summed in bfloat16 or wider, within the bound.
A program may use at most 64 MiB of HBM per device.

v0:
```python
import math

import jax
import jax.numpy as jnp
from jax import lax
from jax.sharding import PartitionSpec as P

norm_eps = 1e-06
masked_score = -1e30


def merged_2(value, axis, join):
    pieces = jax.tree.map(lambda part: lax.all_gather(part, axis), value)
    head = jax.tree.map(lambda part: part[0], pieces)
    tail = jax.tree.map(lambda part: part[1:], pieces)
    so_far, _ = lax.scan(lambda so_far, share: (join(so_far, share), None), head, tail)
    return so_far


def fold_parts(left_part, right_part):
    peak_all = jnp.maximum(left_part[0], right_part[0])
    weight_one = jnp.exp(left_part[0] - peak_all)
    weight_two = jnp.exp(right_part[0] - peak_all)
    total_sum = left_part[1] * weight_one + right_part[1] * weight_two
    merged = left_part[2] * weight_one[..., None] + right_part[2] * weight_two[..., None]
    return (peak_all, total_sum, merged)


def per_device(
    stream,
    gain_in,
    w_query,
    w_key,
    w_value,
    w_forget,
    keys_cache,
    values_cache,
    decay_cache,
    lengths,
    gain_att,
    w_out,
    gain_mlp,
    w_up,
    w_down,
):
    kv_index = lax.axis_index("kv")
    tp_index = lax.axis_index("tp")
    kv_count = lax.axis_size("kv")
    seqs_here, cols_here = stream.shape
    heads_here = keys_cache.shape[1]
    pos_here = keys_cache.shape[2]
    head_dim = keys_cache.shape[3]
    width_all = cols_here * kv_count
    score_scale = 1.0 / math.sqrt(head_dim)
    stream_float = stream.astype(jnp.float32)
    scaled = (stream_float * gain_in.astype(jnp.float32)).astype(jnp.bfloat16)
    square_sum = jnp.sum(stream_float * stream_float, axis=1)
    forget_rows = lax.dynamic_slice(
        w_forget, (kv_index * cols_here, tp_index * heads_here), (cols_here, heads_here)
    )
    part_query = jnp.dot(scaled, w_query, preferred_element_type=jnp.float32)
    part_key = jnp.dot(scaled, w_key, preferred_element_type=jnp.float32)
    part_value = jnp.dot(scaled, w_value, preferred_element_type=jnp.float32)
    part_forget = jnp.dot(scaled, forget_rows, preferred_element_type=jnp.float32)
    part_query, part_key, part_value, part_forget, square_total = lax.psum(
        (part_query, part_key, part_value, part_forget, square_sum), "kv"
    )
    scale_in = lax.rsqrt(square_total / width_all + norm_eps)[:, None]
    queries = (part_query * scale_in).astype(jnp.bfloat16).reshape(seqs_here, heads_here, head_dim)
    key_new = (part_key * scale_in).astype(jnp.bfloat16).reshape(seqs_here, heads_here, head_dim)
    value_new = (
        (part_value * scale_in).astype(jnp.bfloat16).reshape(seqs_here, heads_here, head_dim)
    )
    forget = jax.nn.log_sigmoid(part_forget * scale_in)
    attention_logits = (
        jnp.einsum("shd,shpd->shp", queries, keys_cache, preferred_element_type=jnp.float32)
        * score_scale
    )
    attention_logits = attention_logits + forget[:, :, None] + decay_cache
    cache_positions = kv_index * pos_here + lax.iota(jnp.int32, pos_here)
    live_mask = (cache_positions[None, :] < lengths[:, None])[:, None, :]
    attention_logits = jnp.where(live_mask, attention_logits, masked_score)
    block_peak = jnp.max(attention_logits, axis=2)
    weights = jnp.where(live_mask, jnp.exp(attention_logits - block_peak[..., None]), 0.0)
    block_total = jnp.sum(weights, axis=2)
    block_out = jnp.einsum(
        "shp,shpd->shd",
        weights.astype(jnp.bfloat16),
        values_cache,
        preferred_element_type=jnp.float32,
    )
    peak_all, total_all, out_all = merged_2((block_peak, block_total, block_out), "kv", fold_parts)
    own_score = (
        jnp.sum(queries.astype(jnp.float32) * key_new.astype(jnp.float32), axis=2) * score_scale
    )
    top_score = jnp.maximum(peak_all, own_score)
    past_weight = jnp.exp(peak_all - top_score)
    own_weight = jnp.exp(own_score - top_score)
    numerator = (
        out_all * past_weight[..., None] + value_new.astype(jnp.float32) * own_weight[..., None]
    )
    denominator = total_all * past_weight + own_weight
    attended = (numerator / denominator[..., None]).reshape(seqs_here, heads_here * head_dim)
    attended_in = (attended * gain_att.astype(jnp.float32)).astype(jnp.bfloat16)
    part_out = jnp.dot(attended_in, w_out, preferred_element_type=jnp.float32)
    att_squares = jnp.sum(attended * attended, axis=1)
    part_out, att_total = lax.psum((part_out, att_squares), "tp")
    scale_att = lax.rsqrt(att_total / (attended.shape[1] * lax.axis_size("tp")) + norm_eps)[:, None]
    residual = (stream_float + scale_att * part_out).astype(jnp.bfloat16)
    residual_float = residual.astype(jnp.float32)
    mixer_in = (residual_float * gain_mlp.astype(jnp.float32)).astype(jnp.bfloat16)
    mixer_squares = jnp.sum(residual_float * residual_float, axis=1)
    part_up = jnp.dot(mixer_in, w_up, preferred_element_type=jnp.float32)
    pre_act, mixer_total = lax.psum((part_up, mixer_squares), "kv")
    scale_mixer = lax.rsqrt(mixer_total / width_all + norm_eps)[:, None]
    hidden = jnp.square(jax.nn.relu(pre_act * scale_mixer)).astype(jnp.bfloat16)
    part_down = jnp.dot(hidden, w_down, preferred_element_type=jnp.float32)
    mixer_out = lax.psum(part_down, "tp")
    return (residual_float + mixer_out).astype(jnp.bfloat16)


def solution(mesh):
    in_specs = (
        P(None, "kv"),
        P("kv"),
        P("kv", "tp"),
        P("kv", "tp"),
        P("kv", "tp"),
        P(),
        P(None, "tp", "kv", None),
        P(None, "tp", "kv", None),
        P(None, "tp", "kv"),
        P(),
        P("tp"),
        P("tp", "kv"),
        P("kv"),
        P("kv", "tp"),
        P("tp", "kv"),
    )
    out_specs = P(None, "kv")
    return jax.shard_map(
        per_device, mesh=mesh, in_specs=in_specs, out_specs=out_specs, check_vma=False
    )
```

profile of v0, /device:TPU:0, one launch (start us, length us, event | category | flops | bytes accessed | tf_op | source)
XLA Modules:
  0.0 354.1 jit_solution(7159381375102466569)
XLA Ops:
  6.5 0.7 convert_element_type.61
  7.6 1.6 fusion.28
  9.1 1.9 fusion.26
  11.1 1.9 fusion.32
  13.0 0.8 fusion.18
  13.9 0.8 fusion.30
  14.7 44.0 %all-reduce = (f32[32]{0:T(128)S(1)}, f32[32,8]{0,1:T(8,128)S(1)}) all-reduce(f32[32]{0:T(128)S(1)} %fusion.18, f32[32,8]{0,1:T(8,128)S(1)} %fusion.30), channel_id=1, replica_groups=mesh['kv'=16,'tp'=2] {'kv'}, use_global_device_ids=true, to_apply=%region_2.0 | all-reduce | flops 288 | bytes 2304 | tf_op jit(solution)/shard_map/psum | solution.py:65
  58.9 0.7 broadcast_compare_fusion
  59.6 66.0 %all-reduce.8.cloned.1.call-done = (f32[32,1024]{1,0:T(8,128)}, f32[32,1024]{1,0:T(8,128)}, f32[32,1024]{1,0:T(8,128)}) async-done(((f32[32,1024]{1,0:T(8,128)}, f32[32,1024]{1,0:T(8,128)}, f32[32,1024]{1,0:T(8,128)}), (f32[32,1024]{1,0:T(8,128)}, f32[32,1024]{1,0:T(8,128)}, f32[32,1024]{1,0:T(8,128)})) %all-reduce.8.cloned.1.call-update) | async-done | bytes 393232 | tf_op jit(solution)/shard_map/psum | solution.py:65
  125.6 1.1 convert_bitcast_fusion
  126.8 7.9 %fusion.45 = f32[32,8,1,128]{3,2,1,0:T(1,128)S(1)} fusion(bf16[32,8,128,1]{2,3,1,0:T(2,128)(2,1)S(1)} %reshape.83, bf16[32,8,128,128]{3,2,1,0:T(8,128)(2,1)} %param.23), kind=kOutput, calls=%fused_computation.68 | convolution fusion | flops 8388608 | bytes 8585216 | tf_op jit(solution)/shard_map/shd,shpd->shp/dot_general | solution.py:76
  135.2 2.9 fusion.9
  138.7 39.2 %all-gather.3 = f32[16,32,8]{1,2,0:T(8,128)S(1)} all-gather(f32[1,32,8]{1,2,0:T(8,128)S(1)} %copy.34), channel_id=2, replica_groups=mesh['kv'=16,'tp'=2] {'kv'}, dimensions={0}, use_global_device_ids=true | all-gather | bytes 17408 | tf_op jit(solution)/shard_map/all_gather | solution.py:13
  177.8 36.0 %all-gather.4 = f32[16,32,8]{1,2,0:T(8,128)S(1)} all-gather(f32[1,32,8]{1,2,0:T(8,128)S(1)} %copy.35), channel_id=3, replica_groups=mesh['kv'=16,'tp'=2] {'kv'}, dimensions={0}, use_global_device_ids=true | all-gather | bytes 17408 | tf_op jit(solution)/shard_map/all_gather | solution.py:13
  213.9 1.1 slice.36
  215.5 5.3 %while.14 = (s32[]{:T(128)}, f32[32,8]{0,1:T(8,128)S(1)}, f32[32,8]{0,1:T(8,128)S(1)}, f32[32,8,128]{2,1,0:T(8,128)S(1)}, f32[15,32,8]{1,2,0:T(8,128)S(1)}, /*in...) while((s32[]{:T(128)}, f32[32,8]{0,1:T(8,128)S(1)}, f32[32,8]{0,1:T(8,128)S(1)}, ...), condition=%wide.region_7.8_spmd, body=%wide.region_6.7_spmd.sunk | while | flops 99842 | bytes 407653 | solution.py:16
  221.0 0.6 multiply_reduce_fusion
  221.8 3.5 all-reduce.2
  225.5 4.1 %fusion.23 = f32[32,8192]{1,0:T(8,128)} fusion(bf16[256,8192]{1,0:T(8,128)(2,1)} %param.30, bf16[32,256]{1,0:T(8,128)(2,1)S(1)} %get-tuple-element.73, f32[256]{0:T(256)S(1)} %convert_element_type.76), kind=kOutput, calls=%fused_computation.45 | convolution fusion | flops 134242304 | bytes 5260288 | tf_op jit(solution)/shard_map/dot_general | solution.py:113
  229.6 39.0 %psum.78 = f32[32]{0:T(128)S(1)} all-reduce(f32[32]{0:T(128)S(1)} %get-tuple-element.72), channel_id=1, replica_groups=mesh['kv'=16,'tp'=2] {'kv'}, use_global_device_ids=true, to_apply=%region_16.17 | all-reduce | flops 32 | bytes 256 | tf_op jit(solution)/shard_map/psum | solution.py:114
  268.5 71.6 %all-reduce.6.cloned.1.call-done = f32[32,8192]{1,0:T(8,128)} async-done(((f32[32,8192]{1,0:T(8,128)}), f32[32,8192]{1,0:T(8,128)}) %all-reduce.6.cloned.1.call-update) | async-done | bytes 1048592 | tf_op jit(solution)/shard_map/psum | solution.py:114
  340.2 3.4 fusion.3
  343.6 3.4 psum.79
  347.0 0.6 fusion.22
  (111 shorter events, 7.6 us)
Async XLA Ops:
  6.5 1.1 copy-start
  6.5 119.1 %all-reduce.8.cloned.1.call-start = ((), (), s32[]{:S(2)}) async-start(), calls=%async_computation.2 | async-start | bytes 786432 | tf_op jit(solution)/shard_map/psum | solution.py:65
  13.0 200.8 %all-gather.7.cloned.1.call-start = ((), (), s32[]{:S(2)}) async-start(), calls=%async_computation.1 | async-start | bytes 2228224 | tf_op jit(solution)/shard_map/all_gather | solution.py:13
  126.8 8.0 %copy-start.4 = (f32[32,8,128]{2,1,0:T(8,128)S(1)}, f32[32,8,128]{2,1,0:T(8,128)}, u32[]{:S(2)}) copy-start(f32[32,8,128]{2,1,0:T(8,128)} %param.25) | copy-start | bytes 393220
  126.8 8.4 %copy-start.1 = (bf16[32,8,128,128]{3,2,1,0:T(8,128)(2,1)S(1)}, bf16[32,8,128,128]{3,2,1,0:T(8,128)(2,1)}, u32[]{:S(2)}) copy-start(bf16[32,8,128,128]{3,2,1,0:T(8,128)(2,1)} %param.24) | copy-start | bytes 25165828
  135.2 3.0 copy-start.6
  135.2 3.0 copy-start.5
  138.2 202.0 %all-reduce.6.cloned.1.call-start = ((), (), s32[]{:S(2)}) async-start(), calls=%async_computation | async-start | bytes 2097152 | tf_op jit(solution)/shard_map/psum | solution.py:114
  138.3 83.3 %copy-start.3 = (bf16[1024,256]{1,0:T(8,128)(2,1)S(1)}, bf16[1024,256]{1,0:T(8,128)(2,1)}, u32[]{:S(2)}) copy-start(bf16[1024,256]{1,0:T(8,128)(2,1)} %param.28) | copy-start | bytes 1572868
  177.8 47.5 %copy-start.2 = (bf16[32,256]{1,0:T(8,128)(2,1)S(1)}, bf16[32,256]{1,0:T(8,128)(2,1)}, u32[]{:S(2)}) copy-start(bf16[32,256]{1,0:T(8,128)(2,1)} %param.17) | copy-start | bytes 49156
  213.8 1.6 slice-start
Sparse Core Ops, SparseCore 0:
  13.1 112.4 all-reduce.7
  138.3 59.8 all-gather.6
  229.7 110.4 all-reduce.5
where the time goes:
time: 355 us; the launch traced here: 354 us
  blocking collectives  165 us (46%)
  waiting for transfers between devices  138 us (39%)
  matrix products  24.7 us (7%)
  between operations  13.4 us (4%)
  other arithmetic  8.01 us (2%)
  local copies, waits for them, and re-layouts  4.88 us (1%)
    all_gather x2, blocking collectives, merged_2(): pieces = jax.tree.map(lambda part: lax.all_gather(part, axis), value)  75.1 us
    psum x1, waiting for transfers between devices, per_device(): pre_act, mixer_total = lax.psum((part_up, mixer_squares), 'kv')  71.6 us
    psum x1, waiting for transfers between devices, per_device(): lax.psum((part_query, part_key, part_value, part_forget, square_sum), 'kv')  66 us
    psum x1, blocking collectives, per_device(): lax.psum((part_query, part_key, part_value, part_forget, square_sum), 'kv')  44 us
    psum x1, blocking collectives, per_device(): pre_act, mixer_total = lax.psum((part_up, mixer_squares), 'kv')  39 us
    dot_general x1, matrix products, per_device(): jnp.einsum('shd,shpd->shp', queries, keys_cache, preferred_element_type=j...  7.93 us
  transfers between devices with their start and end apart: 3, of which 2 were waited for; matrix products, arithmetic and copies ran while one was open for 1% of the time, Pallas kernels for 0%

commit v1 on v0

--- a/solution.py
+++ b/solution.py
@@ -1,9 +1,16 @@
+import functools
 import math
 
 import jax
 import jax.numpy as jnp
 from jax import lax
+from jax.experimental import pallas as pl
+from jax.experimental.pallas import tpu as pltpu
 from jax.sharding import PartitionSpec as P
+
+f32 = jnp.float32
+bf16 = jnp.bfloat16
+LANES = 128
 
 norm_eps = 1e-06
 masked_score = -1e30
@@ -119,6 +126,412 @@
     return (residual_float + mixer_out).astype(jnp.bfloat16)
 
 
+def thirds(value, group, wide):
+    high = value.astype(bf16).astype(f32)
+    rest = value - high
+    mid = rest.astype(bf16).astype(f32)
+    low = rest - mid
+    third = group % 3 if wide else group
+    picked = jnp.where(third == 0, high, jnp.where(third == 1, mid, low))
+    return picked
+
+
+def lanes_of(shape):
+    return lax.broadcasted_iota(jnp.int32, shape, len(shape) - 1)
+
+
+def layer_kernel(
+    kv_n, heads_all, pos_here,
+    lengths, stream, gain_in, gain_att, gain_mlp, decay,
+    w_forget, w_query, w_key, w_value, keys, values, w_out, w_up, w_down,
+    out,
+    wf_v, wq_v, wk_v, wv_v, keys_v, values_v, wo_v, wu_v, wd_v,
+    send1, recv1, q_all, q_float, o_float, s_float, send3, recv3, att_all,
+    send5, recv5, send6, recv6, hid_all, send8, recv8,
+    load_sem, cache_sem, ssem, rsem, pair_ssem, pair_rsem,
+):
+    me = lax.axis_index("kv")
+    tp = lax.axis_index("tp")
+    seqs, cols = stream.shape
+    heads = decay.shape[1]
+    dim = keys.shape[-1]
+    rows = send1.shape[1] // 4
+    groups = seqs // rows
+    hidden_here = hid_all.shape[2]
+    others = kv_n - 1
+    chunks = cache_sem.shape[1]
+    per_chunk = seqs // chunks
+    score_scale = 1.0 / math.sqrt(dim)
+
+    def load(src, dst, index):
+        return pltpu.make_async_copy(src, dst, load_sem.at[index])
+
+    start_row = pl.multiple_of(me * cols, cols)
+    first_loads = [
+        load(w_forget.at[pl.ds(start_row, cols), :], wf_v, 0),
+        load(w_query, wq_v, 1),
+        load(w_key, wk_v, 2),
+        load(w_value, wv_v, 3),
+    ]
+    for copy in first_loads:
+        copy.start()
+
+    def cache_copy(which, chunk):
+        src, dst = ((keys, keys_v), (values, values_v))[which]
+        part = pl.ds(chunk * per_chunk, per_chunk)
+        return pltpu.make_async_copy(src.at[part], dst.at[part], cache_sem.at[which, chunk])
+
+    late_loads = [load(w_out, wo_v, 4), load(w_up, wu_v, 5), load(w_down, wd_v, 6)]
+
+    barrier = pltpu.get_barrier_semaphore()
+
+    def greet(k, carry):
+        pl.semaphore_signal(
+            barrier, inc=1, device_id=(lax.rem(me + k, kv_n), tp),
+            device_id_type=pl.DeviceIdType.MESH,
+        )
+        return carry
+
+    lax.fori_loop(1, kv_n, greet, 0)
+    pl.semaphore_signal(
+        barrier, inc=1, device_id=(me, 1 - tp), device_id_type=pl.DeviceIdType.MESH
+    )
+
+    def after(k):
+        return lax.rem(me + k, kv_n)
+
+    def before(k):
+        return lax.rem(me + kv_n - k, kv_n)
+
+    def remote(phase, k, src, dst):
+        return pltpu.make_async_remote_copy(
+            src_ref=src, dst_ref=dst,
+            send_sem=ssem.at[phase, k - 1], recv_sem=rsem.at[phase, k - 1],
+            device_id=(after(k), tp), device_id_type=pl.DeviceIdType.MESH,
+        )
+
+    def scatter(phase, k, send, recv):
+        return remote(phase, k, send.at[after(k)], recv.at[k - 1])
+
+    def spread(phase, k, held):
+        return remote(phase, k, held.at[me], held.at[me])
+
+    def landed(phase, k, held):
+        return remote(phase, k, held.at[before(k)], held.at[before(k)])
+
+    def each(body):
+        lax.fori_loop(1, kv_n, lambda k, carry: (body(k), carry)[1], 0)
+
+    def swap(index, src, dst):
+        return pltpu.make_async_remote_copy(
+            src_ref=src, dst_ref=dst, send_sem=pair_ssem.at[index],
+            recv_sem=pair_rsem.at[index], device_id=(me, 1 - tp),
+            device_id_type=pl.DeviceIdType.MESH,
+        )
+
+    x = stream[...].astype(f32)
+    scaled = (x * gain_in[...].astype(f32)).astype(bf16)
+    squares = jnp.sum(x * x, axis=1, keepdims=True)
+    for copy in first_loads:
+        copy.wait()
+    for chunk in range(chunks):
+        cache_copy(0, chunk).start()
+        cache_copy(1, chunk).start()
+    for copy in late_loads:
+        copy.start()
+    lane = lanes_of((seqs, LANES))
+    expand = lax.broadcasted_iota(jnp.int32, (heads_all, LANES), 0) == (
+        lanes_of((heads_all, LANES)) % 32
+    )
+    wide_forget = jnp.dot(
+        wf_v[...], jnp.where(expand, 1.0, 0.0).astype(bf16), preferred_element_type=f32
+    ).astype(bf16)
+    part_forget = jnp.dot(scaled, wide_forget, preferred_element_type=f32)
+    stats = jnp.where(lane % 32 < heads_all, part_forget, squares)
+    stats = thirds(stats, lane // 32, False)
+    stats = jnp.where(lane < 96, stats, 0.0).astype(bf16)
+    for place, weight in enumerate((wq_v, wk_v, wv_v)):
+        part = jnp.dot(scaled, weight[...], preferred_element_type=f32).astype(bf16)
+        for g in range(groups):
+            for h in range(heads):
+                send1[g * heads + h, place * rows:(place + 1) * rows, :] = part[
+                    g * rows:(g + 1) * rows, h * dim:(h + 1) * dim
+                ]
+    for g in range(groups):
+        for h in range(heads):
+            send1[g * heads + h, 3 * rows:4 * rows, :] = stats[g * rows:(g + 1) * rows]
+    pl.semaphore_wait(barrier, kv_n)
+    each(lambda k: scatter(0, k, send1, recv1).start())
+
+    def add1(k, total):
+        scatter(0, k, send1, recv1).wait_recv()
+        return total + recv1[k - 1].astype(f32)
+
+    total = lax.fori_loop(1, kv_n, add1, send1[me].astype(f32))
+    lane_r = lanes_of((rows, LANES))
+    stat = total[3 * rows:]
+    my_head = tp * heads + lax.rem(me, heads)
+    forget_sum = jnp.sum(
+        jnp.where(lane_r % 32 == my_head, stat, 0.0), axis=1, keepdims=True
+    )
+    square_sum = jnp.sum(
+        jnp.where(lane_r % 32 == heads_all, stat, 0.0), axis=1, keepdims=True
+    )
+    width_all = cols * kv_n
+    scale_in = lax.rsqrt(square_sum / width_all + norm_eps)
+    query = (total[:rows] * scale_in).astype(bf16)
+    key_new = (total[rows:2 * rows] * scale_in).astype(bf16).astype(f32)
+    value_new = (total[2 * rows:3 * rows] * scale_in).astype(bf16).astype(f32)
+    gate = forget_sum * scale_in
+    forget = jnp.minimum(gate, 0.0) - jnp.log1p(jnp.exp(-jnp.abs(gate)))
+    q_all[me] = query
+    each(lambda k: spread(1, k, q_all).start())
+    own_score = (
+        jnp.sum(query.astype(f32) * key_new, axis=1, keepdims=True) * score_scale
+    )
+    each(lambda k: landed(1, k, q_all).wait_recv())
+
+    q_float[...] = q_all[...].reshape(kv_n * rows, dim).astype(f32)
+    head_row = lax.broadcasted_iota(jnp.int32, (heads, pos_here), 0)
+    position = me * pos_here + lanes_of((heads, pos_here))
+    lane_h = lanes_of((heads, LANES))
+
+    def one_sequence(s):
+        first = (s // rows) * (heads * rows) + s % rows
+        mine = pl.ds(first, heads, stride=rows)
+        q_s = q_float[mine, :].astype(bf16)
+        k_s = keys_v[s].reshape(heads * pos_here, dim)
+        every = lax.dot_general(
+            q_s, k_s, (((1,), (1,)), ((), ())), preferred_element_type=f32
+        )
+        score = every[:, :pos_here]
+        for h in range(1, heads):
+            score = jnp.where(
+                head_row == h, every[:, h * pos_here:(h + 1) * pos_here], score
+            )
+        score = score * score_scale + decay[s]
+        live = position < lengths[s]
+        score = jnp.where(live, score, masked_score)
+        peak = jnp.max(score, axis=1, keepdims=True)
+        probs = jnp.where(live, jnp.exp(score - peak), 0.0)
+        block_total = jnp.sum(probs, axis=1, keepdims=True)
+        spread_probs = jnp.concatenate(
+            [jnp.where(head_row == h, probs, 0.0) for h in range(heads)], axis=1
+        ).astype(bf16)
+        v_s = values_v[s].reshape(heads * pos_here, dim)
+        o_float[mine, :] = jnp.dot(spread_probs, v_s, preferred_element_type=f32)
+        s_float[mine, :] = jnp.where(lane_h < 48, peak, block_total)
+
+    def one_chunk(chunk, carry):
+        cache_copy(0, chunk).wait()
+        cache_copy(1, chunk).wait()
+
+        def inner(i, c):
+            one_sequence(chunk * per_chunk + 2 * i)
+            one_sequence(chunk * per_chunk + 2 * i + 1)
+            return c
+
+        return lax.fori_loop(0, per_chunk // 2, inner, carry)
+
+    lax.fori_loop(0, chunks, one_chunk, 0)
+    stats3 = s_float[...]
+    stats3 = thirds(stats3, lanes_of(stats3.shape) // 16, True)
+    send3[:, :rows, :] = o_float[...].astype(bf16).reshape(kv_n, rows, dim)
+    send3[:, rows:, :] = stats3.astype(bf16).reshape(kv_n, rows, LANES)
+    each(lambda k: scatter(2, k, send3, recv3).start())
+
+    def opened(block):
+        wide = block.astype(f32)
+        stat = wide[rows:]
+        is_third = lane_r % 16 == 0
+        peak = jnp.sum(
+            jnp.where(is_third & (lane_r < 48), stat, 0.0), axis=1, keepdims=True
+        )
+        total = jnp.sum(
+            jnp.where(is_third & (lane_r >= 48) & (lane_r < 96), stat, 0.0),
+            axis=1, keepdims=True,
+        )
+        return peak, total, wide[:rows]
+
+    def fold3(k, so_far):
+        scatter(2, k, send3, recv3).wait_recv()
+        peak_a, total_a, out_a = so_far
+        peak_b, total_b, out_b = opened(recv3[k - 1])
+        peak = jnp.maximum(peak_a, peak_b)
+        one, two = jnp.exp(peak_a - peak), jnp.exp(peak_b - peak)
+        return peak, total_a * one + total_b * two, out_a * one + out_b * two
+
+    peak_all, total_all, out_all = lax.fori_loop(1, kv_n, fold3, opened(send3[me]))
+    peak_all = peak_all + forget
+    top = jnp.maximum(peak_all, own_score)
+    past_weight = jnp.exp(peak_all - top)
+    own_weight = jnp.exp(own_score - top)
+    att_all[me] = (out_all * past_weight + value_new * own_weight) / (
+        total_all * past_weight + own_weight
+    )
+    each(lambda k: spread(3, k, att_all).start())
+    each(lambda k: landed(3, k, att_all).wait_recv())
+    attended = jnp.concatenate(
+        [
+            jnp.concatenate([att_all[g * heads + h] for g in range(groups)], axis=0)
+            for h in range(heads)
+        ],
+        axis=1,
+    )
+    attended_in = (attended * gain_att[...].astype(f32)).astype(bf16)
+    late_loads[0].wait()
+    part_out = jnp.dot(attended_in, wo_v[...], preferred_element_type=f32)
+    att_squares = jnp.sum(attended * attended, axis=1, keepdims=True)
+    send5[:, :cols] = part_out
+    send5[:, cols:] = jnp.broadcast_to(att_squares, (seqs, LANES))
+    swap5 = swap(0, send5, recv5)
+    swap5.start()
+    late_loads[1].wait()
+    swap5.wait_recv()
+    scale_att = lax.rsqrt(
+        (att_squares + recv5[:, cols:cols + 1]) / (attended.shape[1] * 2) + norm_eps
+    )
+    residual = (
+        stream[...].astype(f32) + scale_att * (part_out + recv5[:, :cols])
+    ).astype(bf16).astype(f32)
+    mixer_in = (residual * gain_mlp[...].astype(f32)).astype(bf16)
+    mixer_squares = jnp.sum(residual * residual, axis=1, keepdims=True)
+    mixer_stats = thirds(jnp.broadcast_to(mixer_squares, (seqs, LANES)), lane, False)
+    mixer_stats = jnp.where(lane < 3, mixer_stats, 0.0).astype(bf16)
+
+    def up(owner):
+        columns = pl.ds(pl.multiple_of(owner * hidden_here, LANES), hidden_here)
+        send6[owner, :, :hidden_here] = jnp.dot(
+            mixer_in, wu_v[:, columns], preferred_element_type=f32
+        ).astype(bf16)
+        send6[owner, :, hidden_here:] = mixer_stats
+
+    def up_send(k):
+        up(after(k))
+        scatter(4, k, send6, recv6).start()
+
+    each(up_send)
+    up(me)
+
+    def add6(k, total):
+        scatter(4, k, send6, recv6).wait_recv()
+        return total + recv6[k - 1].astype(f32)
+
+    pre_act = lax.fori_loop(1, kv_n, add6, send6[me].astype(f32))
+    mixer_total = jnp.sum(pre_act[:, hidden_here:], axis=1, keepdims=True)
+    scale_mixer = lax.rsqrt(mixer_total / width_all + norm_eps)
+    hidden = jnp.maximum(pre_act[:, :hidden_here] * scale_mixer, 0.0)
+    hid_all[me] = (hidden * hidden).astype(bf16)
+    each(lambda k: spread(5, k, hid_all).start())
+    late_loads[2].wait()
+
+    def down(owner):
+        depth = pl.ds(pl.multiple_of(owner * hidden_here, LANES), hidden_here)
+        return jnp.dot(hid_all[owner], wd_v[depth, :], preferred_element_type=f32)
+
+    def add7(k, total):
+        landed(5, k, hid_all).wait_recv()
+        return total + down(before(k))
+
+    part_down = lax.fori_loop(1, kv_n, add7, down(me))
+    send8[...] = part_down
+    swap8 = swap(1, send8, recv8)
+    swap8.start()
+    swap8.wait_recv()
+    out[...] = (residual + (part_down + recv8[...])).astype(bf16)
+
+    def drain(k):
+        scatter(0, k, send1, recv1).wait_send()
+        spread(1, k, q_all).wait_send()
+        scatter(2, k, send3, recv3).wait_send()
+        spread(3, k, att_all).wait_send()
+        scatter(4, k, send6, recv6).wait_send()
+        spread(5, k, hid_all).wait_send()
+
+    each(drain)
+    swap5.wait_send()
+    swap8.wait_send()
+
+
+def fits(kv_n, tp_n, seqs, cols, heads, heads_all, pos_here, dim, units):
+    if tp_n != 2 or heads != 8 or (seqs * heads) % kv_n or units % kv_n:
+        return False
+    rows = seqs * heads // kv_n
+    return (
+        rows % 16 == 0 and seqs % rows == 0 and seqs % 16 == 0 and cols % LANES == 0
+        and pos_here == LANES and dim == LANES and heads_all <= 16
+        and (units // kv_n) % LANES == 0
+    )
+
+
+def layer(
+    stream, gain_in, w_query, w_key, w_value, w_forget, keys_cache, values_cache,
+    decay_cache, lengths, gain_att, w_out, gain_mlp, w_up, w_down,
+):
+    kv_n, tp_n = lax.axis_size("kv"), lax.axis_size("tp")
+    seqs, cols = stream.shape
+    heads, pos_here, dim = keys_cache.shape[1:]
+    heads_all = w_forget.shape[1]
+    units = w_up.shape[1]
+    if not fits(kv_n, tp_n, seqs, cols, heads, heads_all, pos_here, dim, units):
+        return per_device(
+            stream, gain_in, w_query, w_key, w_value, w_forget, keys_cache, values_cache,
+            decay_cache, lengths, gain_att, w_out, gain_mlp, w_up, w_down,
+        )
+    rows = seqs * heads // kv_n
+    hidden_here = units // kv_n
+    others = kv_n - 1
+    chunks = 4 if seqs % 8 == 0 else 1
+    vmem = pl.BlockSpec(memory_space=pltpu.VMEM)
+    anywhere = pl.BlockSpec(memory_space=pl.ANY)
+    return pl.pallas_call(
+        functools.partial(layer_kernel, kv_n, heads_all, pos_here),
+        out_shape=jax.ShapeDtypeStruct((seqs, cols), bf16),
+        in_specs=[pl.BlockSpec(memory_space=pltpu.SMEM)] + [vmem] * 5 + [anywhere] * 9,
+        out_specs=vmem,
+        scratch_shapes=[
+            pltpu.VMEM((cols, heads_all), bf16),
+            pltpu.VMEM(w_query.shape, bf16),
+            pltpu.VMEM(w_key.shape, bf16),
+            pltpu.VMEM(w_value.shape, bf16),
+            pltpu.VMEM(keys_cache.shape, bf16),
+            pltpu.VMEM(values_cache.shape, bf16),
+            pltpu.VMEM(w_out.shape, bf16),
+            pltpu.VMEM(w_up.shape, bf16),
+            pltpu.VMEM(w_down.shape, bf16),
+            pltpu.VMEM((kv_n, 4 * rows, dim), bf16),
+            pltpu.VMEM((others, 4 * rows, dim), bf16),
+            pltpu.VMEM((kv_n, rows, dim), bf16),
+            pltpu.VMEM((kv_n * rows, dim), f32),
+            pltpu.VMEM((kv_n * rows, dim), f32),
+            pltpu.VMEM((kv_n * rows, LANES), f32),
+            pltpu.VMEM((kv_n, 2 * rows, dim), bf16),
+            pltpu.VMEM((others, 2 * rows, dim), bf16),
+            pltpu.VMEM((kv_n, rows, dim), f32),
+            pltpu.VMEM((seqs, cols + LANES), f32),
+            pltpu.VMEM((seqs, cols + LANES), f32),
+            pltpu.VMEM((kv_n, seqs, hidden_here + LANES), bf16),
+            pltpu.VMEM((others, seqs, hidden_here + LANES), bf16),
+            pltpu.VMEM((kv_n, seqs, hidden_here), bf16),
+            pltpu.VMEM((seqs, cols), f32),
+            pltpu.VMEM((seqs, cols), f32),
+            pltpu.SemaphoreType.DMA((7,)),
+            pltpu.SemaphoreType.DMA((2, chunks)),
+            pltpu.SemaphoreType.DMA((6, others)),
+            pltpu.SemaphoreType.DMA((6, others)),
+            pltpu.SemaphoreType.DMA((2,)),
+            pltpu.SemaphoreType.DMA((2,)),
+        ],
+        compiler_params=pltpu.CompilerParams(
+            collective_id=0, has_side_effects=True, vmem_limit_bytes=60 * 1024 * 1024
+        ),
+    )(
+        lengths, stream, gain_in.reshape(1, -1), gain_att.reshape(1, -1),
+        gain_mlp.reshape(1, -1), decay_cache,
+        w_forget, w_query, w_key, w_value, keys_cache, values_cache, w_out, w_up, w_down,
+    )
+
+
 def solution(mesh):
     in_specs = (
         P(None, "kv"),
@@ -139,5 +552,5 @@
     )
     out_specs = P(None, "kv")
     return jax.shard_map(
-        per_device, mesh=mesh, in_specs=in_specs, out_specs=out_specs, check_vma=False
-    )
+        layer, mesh=mesh, in_specs=in_specs, out_specs=out_specs, check_vma=False
+    )

time: 355 us -> 84.2 us (0.24)
  the two profiles are of different devices: /device:TPU:0 before, /device:TPU:29 now
where the time goes in v1:
time: 84.2 us; the launch traced here: 84 us
  Pallas kernels  76.6 us (91%)
  local copies, waits for them, and re-layouts  7.3 us (9%)
    pallas_call x1, Pallas kernels, layer(): pl.pallas_call(functools.partial(layer_kernel, kv_n, heads_all, pos_here)...  76.6 us
    unnamed x2, local copies, waits for them, and re-layouts  3.56 us

profile of v1, /device:TPU:29, one launch (start us, length us, event | category | flops | bytes accessed | tf_op | source)
XLA Modules:
  0.0 84.0 jit_solution(13524346828713764663)
XLA Ops:
  0.0 1.2 %reshape.9.gain_in = bf16[1,256]{1,0:T(2,128)(2,1)} reshape(bf16[256]{0:T(256)(128)(2,1)} %param.16) | data formatting | bytes 1024 | tf_op jit(solution)/shard_map/reshape | solution.py:529
  1.2 1.2 %reshape.11.gain_mlp = bf16[1,256]{1,0:T(2,128)(2,1)} reshape(bf16[256]{0:T(256)(128)(2,1)} %param.27) | data formatting | bytes 1024 | tf_op jit(solution)/shard_map/reshape | solution.py:530
  2.5 1.3 %reshape.10.gain_att = bf16[1,1024]{1,0:T(2,128)(2,1)} reshape(bf16[1024]{0:T(1024)(128)(2,1)} %param.25) | data formatting | bytes 4096 | tf_op jit(solution)/shard_map/reshape | solution.py:529
  3.7 2.2 %copy.16.w_forget = bf16[4096,16]{1,0:T(8,128)(2,1)} copy(bf16[4096,16]{0,1:T(8,128)(2,1)} %param.20) | data formatting | bytes 262144 | tf_op args[5]
  6.0 76.6 %shard_map.145 = bf16[32,256]{1,0:T(8,128)(2,1)} custom-call(s32[32]{0:T(128)} %lengths.1, bf16[32,256]{1,0:T(8,128)(2,1)} %stream.1, bf16[1,256]{1,0:T(2,128)(2,1)} %reshape.9.gain_in, bf16[1,1024]{1,0:T(2,128)(2,1)} %reshape.10.gain_att, bf16[1,256]{1,0:T(2,128)(2,1)} %reshape.11.gain_mlp, f32[32,8,128]{2,1,0:T(8,128)} %decay.1, ...), custom_call_target="tpu_custom_call" | custom-call | tf_op jit(solution)/shard_map/pallas_call | solution.py:487
  82.6 1.3 %copy.18 = bf16[32,256]{1,0:T(8,128)(2,1)} copy(bf16[32,256]{1,0:T(8,128)(2,1)} %shard_map.145) | data formatting | bytes 32768

commit v2 on v1

--- a/solution.py
+++ b/solution.py
@@ -162,13 +162,14 @@
     chunks = cache_sem.shape[1]
     per_chunk = seqs // chunks
     score_scale = 1.0 / math.sqrt(dim)
+    together = math.gcd(8, per_chunk)
 
     def load(src, dst, index):
         return pltpu.make_async_copy(src, dst, load_sem.at[index])
 
     start_row = pl.multiple_of(me * cols, cols)
     first_loads = [
-        load(w_forget.at[pl.ds(start_row, cols), :], wf_v, 0),
+        load(w_forget.at[:, pl.ds(start_row, cols)], wf_v, 0),
         load(w_query, wq_v, 1),
         load(w_key, wk_v, 2),
         load(w_value, wv_v, 3),
@@ -197,11 +198,12 @@
         barrier, inc=1, device_id=(me, 1 - tp), device_id_type=pl.DeviceIdType.MESH
     )
 
-    def after(k):
-        return lax.rem(me + k, kv_n)
-
-    def before(k):
-        return lax.rem(me + kv_n - k, kv_n)
+    def partner(k):
+        apart = kv_n - k
+        bits = [1 << place for place in range(kv_n.bit_length() - 1)]
+        return sum((((me // bit) + (apart // bit)) % 2) * bit for bit in bits)
+
+    after = before = partner
 
     def remote(phase, k, src, dst):
         return pltpu.make_async_remote_copy(
@@ -230,7 +232,7 @@
         )
 
     x = stream[...].astype(f32)
-    scaled = (x * gain_in[...].astype(f32)).astype(bf16)
+    scaled = (x * gain_in[...].astype(f32).reshape(1, -1)).astype(bf16)
     squares = jnp.sum(x * x, axis=1, keepdims=True)
     for copy in first_loads:
         copy.wait()
@@ -243,8 +245,9 @@
     expand = lax.broadcasted_iota(jnp.int32, (heads_all, LANES), 0) == (
         lanes_of((heads_all, LANES)) % 32
     )
-    wide_forget = jnp.dot(
-        wf_v[...], jnp.where(expand, 1.0, 0.0).astype(bf16), preferred_element_type=f32
+    wide_forget = lax.dot_general(
+        wf_v[...], jnp.where(expand, 1.0, 0.0).astype(bf16), (((0,), (0,)), ((), ())),
+        preferred_element_type=f32,
     ).astype(bf16)
     part_forget = jnp.dot(scaled, wide_forget, preferred_element_type=f32)
     stats = jnp.where(lane % 32 < heads_all, part_forget, squares)
@@ -296,42 +299,55 @@
     position = me * pos_here + lanes_of((heads, pos_here))
     lane_h = lanes_of((heads, LANES))
 
-    def one_sequence(s):
-        first = (s // rows) * (heads * rows) + s % rows
-        mine = pl.ds(first, heads, stride=rows)
-        q_s = q_float[mine, :].astype(bf16)
-        k_s = keys_v[s].reshape(heads * pos_here, dim)
-        every = lax.dot_general(
-            q_s, k_s, (((1,), (1,)), ((), ())), preferred_element_type=f32
-        )
-        score = every[:, :pos_here]
-        for h in range(1, heads):
-            score = jnp.where(
-                head_row == h, every[:, h * pos_here:(h + 1) * pos_here], score
+    def some_sequences(first_seq):
+        batch = [first_seq + i for i in range(together)]
+        places = [
+            pl.ds((s // rows) * (heads * rows) + s % rows, heads, stride=rows) for s in batch
+        ]
+        q_parts = [q_float[mine, :].astype(bf16) for mine in places]
+        everies = [
+            lax.dot_general(
+                q_s, keys_v[s].reshape(heads * pos_here, dim), (((1,), (1,)), ((), ())),
+                preferred_element_type=f32,
             )
-        score = score * score_scale + decay[s]
-        live = position < lengths[s]
-        score = jnp.where(live, score, masked_score)
-        peak = jnp.max(score, axis=1, keepdims=True)
-        probs = jnp.where(live, jnp.exp(score - peak), 0.0)
-        block_total = jnp.sum(probs, axis=1, keepdims=True)
-        spread_probs = jnp.concatenate(
-            [jnp.where(head_row == h, probs, 0.0) for h in range(heads)], axis=1
-        ).astype(bf16)
-        v_s = values_v[s].reshape(heads * pos_here, dim)
-        o_float[mine, :] = jnp.dot(spread_probs, v_s, preferred_element_type=f32)
-        s_float[mine, :] = jnp.where(lane_h < 48, peak, block_total)
+            for q_s, s in zip(q_parts, batch)
+        ]
+        spreads, stats = [], []
+        for every, s in zip(everies, batch):
+            score = every[:, :pos_here]
+            for h in range(1, heads):
+                score = jnp.where(
+                    head_row == h, every[:, h * pos_here:(h + 1) * pos_here], score
+                )
+            score = score * score_scale + decay[s]
+            live = position < lengths[s]
+            score = jnp.where(live, score, masked_score)
+            peak = jnp.max(score, axis=1, keepdims=True)
+            probs = jnp.where(live, jnp.exp(score - peak), 0.0)
+            block_total = jnp.sum(probs, axis=1, keepdims=True)
+            spreads.append(jnp.concatenate(
+                [jnp.where(head_row == h, probs, 0.0) for h in range(heads)], axis=1
+            ).astype(bf16))
+            stats.append(jnp.where(lane_h < 48, peak, block_total))
+        outs = [
+            jnp.dot(
+                part, values_v[s].reshape(heads * pos_here, dim), preferred_element_type=f32
+            )
+            for part, s in zip(spreads, batch)
+        ]
+        for mine, out_s, stat_s in zip(places, outs, stats):
+            o_float[mine, :] = out_s
+            s_float[mine, :] = stat_s
 
     def one_chunk(chunk, carry):
         cache_copy(0, chunk).wait()
         cache_copy(1, chunk).wait()
 
         def inner(i, c):
-            one_sequence(chunk * per_chunk + 2 * i)
-            one_sequence(chunk * per_chunk + 2 * i + 1)
+            some_sequences(chunk * per_chunk + together * i)
             return c
 
-        return lax.fori_loop(0, per_chunk // 2, inner, carry)
+        return lax.fori_loop(0, per_chunk // together, inner, carry)
 
     lax.fori_loop(0, chunks, one_chunk, 0)
     stats3 = s_float[...]
@@ -378,7 +394,7 @@
         ],
         axis=1,
     )
-    attended_in = (attended * gain_att[...].astype(f32)).astype(bf16)
+    attended_in = (attended * gain_att[...].astype(f32).reshape(1, -1)).astype(bf16)
     late_loads[0].wait()
     part_out = jnp.dot(attended_in, wo_v[...], preferred_element_type=f32)
     att_squares = jnp.sum(attended * attended, axis=1, keepdims=True)
@@ -394,7 +410,7 @@
     residual = (
         stream[...].astype(f32) + scale_att * (part_out + recv5[:, :cols])
     ).astype(bf16).astype(f32)
-    mixer_in = (residual * gain_mlp[...].astype(f32)).astype(bf16)
+    mixer_in = (residual * gain_mlp[...].astype(f32).reshape(1, -1)).astype(bf16)
     mixer_squares = jnp.sum(residual * residual, axis=1, keepdims=True)
     mixer_stats = thirds(jnp.broadcast_to(mixer_squares, (seqs, LANES)), lane, False)
     mixer_stats = jnp.where(lane < 3, mixer_stats, 0.0).astype(bf16)
@@ -454,11 +470,12 @@
 
 
 def fits(kv_n, tp_n, seqs, cols, heads, heads_all, pos_here, dim, units):
-    if tp_n != 2 or heads != 8 or (seqs * heads) % kv_n or units % kv_n:
+    if tp_n != 2 or heads != 8 or (seqs * heads) % kv_n or units % kv_n or seqs % 32:
         return False
     rows = seqs * heads // kv_n
     return (
-        rows % 16 == 0 and seqs % rows == 0 and seqs % 16 == 0 and cols % LANES == 0
+        rows % 16 == 0 and 4 % max(1, seqs // rows) == 0 and seqs % rows == 0
+        and kv_n & (kv_n - 1) == 0 and cols % LANES == 0
         and pos_here == LANES and dim == LANES and heads_all <= 16
         and (units // kv_n) % LANES == 0
     )
@@ -481,7 +498,7 @@
     rows = seqs * heads // kv_n
     hidden_here = units // kv_n
     others = kv_n - 1
-    chunks = 4 if seqs % 8 == 0 else 1
+    chunks = 4
     vmem = pl.BlockSpec(memory_space=pltpu.VMEM)
     anywhere = pl.BlockSpec(memory_space=pl.ANY)
     return pl.pallas_call(
@@ -490,7 +507,7 @@
         in_specs=[pl.BlockSpec(memory_space=pltpu.SMEM)] + [vmem] * 5 + [anywhere] * 9,
         out_specs=vmem,
         scratch_shapes=[
-            pltpu.VMEM((cols, heads_all), bf16),
+            pltpu.VMEM((heads_all, cols), bf16),
             pltpu.VMEM(w_query.shape, bf16),
             pltpu.VMEM(w_key.shape, bf16),
             pltpu.VMEM(w_value.shape, bf16),
@@ -526,9 +543,9 @@
             collective_id=0, has_side_effects=True, vmem_limit_bytes=60 * 1024 * 1024
         ),
     )(
-        lengths, stream, gain_in.reshape(1, -1), gain_att.reshape(1, -1),
-        gain_mlp.reshape(1, -1), decay_cache,
-        w_forget, w_query, w_key, w_value, keys_cache, values_cache, w_out, w_up, w_down,
+        lengths, stream, gain_in, gain_att,
+        gain_mlp, decay_cache,
+        w_forget.T, w_query, w_key, w_value, keys_cache, values_cache, w_out, w_up, w_down,
     )
 
 

time: 84.2 us -> 68.8 us (0.82)
  the two profiles are of different devices: /device:TPU:29 before, /device:TPU:0 now
where the time goes in v2:
time: 68.8 us; the launch traced here: 68.5 us
  Pallas kernels  67.2 us (98%)
  local copies, waits for them, and re-layouts  1.32 us (2%)
    pallas_call x1, Pallas kernels, layer(): pl.pallas_call(functools.partial(layer_kernel, kv_n, heads_all, pos_here)...  67.2 us

profile of v2, /device:TPU:0, one launch (start us, length us, event | category | flops | bytes accessed | tf_op | source)
XLA Modules:
  0.0 68.5 jit_solution(14243189732407616436)
XLA Ops:
  0.0 67.2 %shard_map.145 = bf16[32,256]{1,0:T(8,128)(2,1)} custom-call(s32[32]{0:T(128)} %lengths.1, bf16[32,256]{1,0:T(8,128)(2,1)} %stream.1, bf16[256]{0:T(256)(128)(2,1)} %gain_in.1, bf16[1024]{0:T(1024)(128)(2,1)} %gain_att.1, bf16[256]{0:T(256)(128)(2,1)} %gain_mlp.1, f32[32,8,128]{2,1,0:T(8,128)} %decay.1, bf16[16,4096]{1,0:T(8,128)(2,1)} %bitcast.1, ...), custom_call_target="tpu_custom_call" | custom-call | tf_op jit(solution)/shard_map/pallas_call | solution.py:504
  67.2 1.3 %copy.17 = bf16[32,256]{1,0:T(8,128)(2,1)} copy(bf16[32,256]{1,0:T(8,128)(2,1)} %shard_map.145) | data formatting | bytes 32768
